TPU v7x, 256 devices: a 4x2x16 block of a 4x16x16 slice. The times are simulated.
256 devices in a mesh: grp: 2 (over y), ep: 32 (over z, core), tp: 4 (over x).
Axes of the slice: x: 4, y: 2, z: 16, core: 2. Of those that a mesh axis runs over, the one named last changes fastest.
The devices are a block of a 4x16x16 slice.
Arguments:
- queries: bfloat16 [24576, 1024], P(('grp', 'ep'), 'tp'), parts along dimension 0, may hold values from -6 to 6
- key_values: bfloat16 [24576, 512], P(('grp', 'ep'), 'tp'), parts along dimension 0, may hold values from -6 to 6
- query_gain: float32 [64], replicated, may hold values from 0.5 to 5
- key_gain: float32 [64], replicated, may hold values from 0.5 to 5
- out_weight: bfloat16 [1024, 2048], P('tp'), may hold values from -0.1875 to 0.1875
- second_batch: bfloat16 [32768, 2048], P(('grp', 'ep', 'tp')), parts along dimension 0, may hold values from -6 to 6
- norm_gain: float32 [2048], replicated, may hold values from 0.1 to 1.9
- routes: int32 [32768, 2], P(('grp', 'ep', 'tp')), parts along dimension 0, may hold values from 0 to 63, all different within a row; in each aligned block of 128 rows (0 to 127, 128 to 255, ...) at most 6 rows name the same one
- route_weights: float32 [32768, 2], P(('grp', 'ep', 'tp')), parts along dimension 0, may hold values from 0.2 to 1
- expert_gate: bfloat16 [64, 2048, 1024], P('ep', None, 'tp'), may hold values from -0.125 to 0.125
- expert_up: bfloat16 [64, 2048, 1024], P('ep', None, 'tp'), may hold values from -0.125 to 0.125
- expert_down: bfloat16 [64, 1024, 2048], P('ep', 'tp'), may hold values from -0.1875 to 0.1875
- shared_gate: bfloat16 [2048, 512], P(None, 'tp'), may hold values from -0.125 to 0.125
- shared_up: bfloat16 [2048, 512], P(None, 'tp'), may hold values from -0.125 to 0.125
- shared_down: bfloat16 [512, 2048], P('tp'), may hold values from -0.25 to 0.25
Outputs:
- mixer_out: bfloat16 [24576, 2048], P(('grp', 'ep', 'tp')), parts along dimension 0
- channel_out: bfloat16 [32768, 2048], P(('grp', 'ep', 'tp')), parts along dimension 0
There are 2 independent parts, one for each index of `grp`. A program takes and returns all parts, laid end to end along the dimension named above; an argument that names none is the same for every part. Nothing has to cross between parts.
Inputs may be any that keep to these rules, and one draw needn't show every extreme that they name: `routes`: each row names 2 different experts. Among the rows of one device no expert is named more than 6 times, and in every draw some expert is named exactly 6 times by the rows of some device.
All inputs are finite; a program needn't handle non-finite values.
Results may differ from a plain program's by a relative error of at most 0.015.
The roundings to bfloat16 on the way count: a program that leaves them out, or rounds other values in their place, can miss the bound.
Values may be sent and summed in bfloat16 or wider, within the bound.
A program may use at most 128 MiB of HBM per device.

v0:
```python
import jax
import jax.numpy as jnp
from jax import lax
from jax.sharding import Mesh
from jax.sharding import PartitionSpec as P

GRID_W = 64
EP = ("ep_0", "ep_1")
GRP_EP = ("grp", "ep_0", "ep_1")
GRP_EP_TP = ("grp", "ep_0", "ep_1", "tp")
rope_base = 10000.0
norm_eps = 1e-06


def joined_along(tiles, dim):
    shape = list(tiles.shape[1:])
    shape[dim] *= tiles.shape[0]
    return jnp.moveaxis(tiles, 0, dim).reshape(shape)


def stacked_from(shard, axes, order):
    tiles = shard
    for k in order:
        tiles = lax.all_gather(tiles, axes[k])
    done = order[::-1]
    back = [done.index(k) for k in range(len(axes))]
    tiles = tiles.transpose(*back, *range(len(axes), tiles.ndim))
    return tiles.reshape(-1, *shard.shape)


def whole_of(shard, axes, order, dim):
    return joined_along(stacked_from(shard, axes, order), dim)


def from_everyone(shard, axis):
    copies = jnp.broadcast_to(shard, (lax.axis_size(axis), *shard.shape))
    return lax.all_to_all(copies, axis, split_axis=0, concat_axis=0, tiled=True)


def gathered_copies(shard, axis, dim):
    return joined_along(from_everyone(shard, axis), dim)


def in_blocks(shard, dim, length):
    shape = shard.shape
    tiles = shard.reshape(*shape[:dim], length, shape[dim] // length, *shape[dim + 1 :])
    return jnp.moveaxis(tiles, dim, 0)


def summed_on_arrival(shard, axis, dim):
    tiles = in_blocks(shard, dim, lax.axis_size(axis))
    arrived = lax.all_to_all(tiles, axis, split_axis=0, concat_axis=0, tiled=True)
    return arrived.astype(jnp.float32).sum(axis=0)


def head_norm(vectors, gain):
    return (
        vectors * lax.rsqrt(jnp.mean(vectors * vectors, axis=-1, keepdims=True) + norm_eps) * gain
    )


def turn_heads(vectors, positions):
    row_count, head_count, head_size = vectors.shape
    half_size = head_size // 2
    inverse = rope_base ** (-jnp.arange(0, half_size, 2, dtype=jnp.float32) / half_size)
    grid_row = (positions // GRID_W).astype(jnp.float32)
    grid_column = (positions % GRID_W).astype(jnp.float32)
    angles = jnp.concatenate([grid_row[:, None] * inverse, grid_column[:, None] * inverse], axis=-1)
    cosine = jnp.cos(angles)[:, None, :]
    sine = jnp.sin(angles)[:, None, :]
    paired = vectors.reshape(row_count, head_count, half_size, 2)
    first = paired[..., 0]
    second = paired[..., 1]
    turned = jnp.stack([first * cosine - second * sine, first * sine + second * cosine], axis=-1)
    return turned.reshape(vectors.shape)


def slot_ids(route_rows, expert_count, capacity):
    row_count, top_count = route_rows.shape
    flat_routes = route_rows.reshape(-1)
    onehot = (flat_routes[:, None] == jnp.arange(expert_count, dtype=jnp.int32)[None, :]).astype(
        jnp.int32
    )
    earlier = jnp.cumsum(onehot, axis=0) - onehot
    within = jnp.sum(earlier * onehot, axis=1)
    return (flat_routes * capacity + within).reshape(row_count, top_count)


def slot_table(slots, slot_count):
    row_count, top_count = slots.shape
    flat_slots = slots.reshape(-1)
    owner_row = jnp.arange(row_count * top_count, dtype=jnp.int32) // top_count
    matches = flat_slots[None, :] == jnp.arange(slot_count, dtype=jnp.int32)[:, None]
    occupied = jnp.any(matches, axis=1)
    source_row = jnp.sum(jnp.where(matches, owner_row[None, :], 0), axis=1)
    return jnp.where(occupied, source_row, row_count)


def pick_block(row_count):
    for candidate in range(min(row_count, 1024), 0, -1):
        if row_count % candidate == 0:
            return candidate
    return row_count


def attend_keys(query_turned, scale, running, pieces):
    head_size = query_turned.shape[-1]
    key_block = pick_block(pieces.shape[0])
    blocks = pieces.reshape(pieces.shape[0] // key_block, key_block, 2 * head_size)

    def one_block(carried, block_rows):
        top_now, total_now, acc_now = carried
        scores = (
            jnp.einsum(
                "qhd,kd->hqk",
                query_turned,
                block_rows[:, :head_size],
                preferred_element_type=jnp.float32,
            )
            * scale
        )
        top_new = jnp.maximum(top_now, jnp.max(scores, axis=-1))
        shrink = jnp.exp(top_now - top_new)
        exps = jnp.exp(scores - top_new[..., None])
        total_new = total_now * shrink + jnp.sum(exps, axis=-1)
        acc_new = acc_now * shrink[..., None] + jnp.einsum(
            "hqk,kd->hqd",
            exps.astype(jnp.bfloat16),
            block_rows[:, head_size:],
            preferred_element_type=jnp.float32,
        )
        return ((top_new, total_new, acc_new), None)

    result, ignored = lax.scan(one_block, running, blocks)
    return result


def shared_hidden_of(token_rows, gate_weights, up_weights):
    gate_part = jnp.dot(token_rows, gate_weights, preferred_element_type=jnp.float32)
    up_part = jnp.dot(token_rows, up_weights, preferred_element_type=jnp.float32)
    return (jax.nn.silu(gate_part) * up_part).astype(jnp.bfloat16)


def expert_hidden(slot_rows, gate_weights, up_weights):
    gate_part = jnp.einsum(
        "osjcd,jdf->osjcf", slot_rows, gate_weights, preferred_element_type=jnp.float32
    )
    up_part = jnp.einsum(
        "osjcd,jdf->osjcf", slot_rows, up_weights, preferred_element_type=jnp.float32
    )
    return (jax.nn.silu(gate_part) * up_part).astype(jnp.bfloat16)


def body(
    queries,
    key_values,
    query_gain,
    key_gain,
    out_weight,
    second_batch,
    norm_gain,
    routes,
    route_weights,
    expert_gate,
    expert_up,
    expert_down,
    shared_gate,
    shared_up,
    shared_down,
):
    query_rows = queries.shape[0]
    head_size = query_gain.shape[0]
    heads_here = queries.shape[1] // head_size
    ep_count = lax.axis_size(EP)
    positions = lax.axis_index(EP) * query_rows + jnp.arange(query_rows, dtype=jnp.int32)
    query_turned = turn_heads(
        head_norm(
            queries.reshape(query_rows, heads_here, head_size).astype(jnp.float32), query_gain
        ),
        positions,
    ).astype(jnp.bfloat16)
    key_turned = turn_heads(
        head_norm(key_values[:, None, :head_size].astype(jnp.float32), key_gain), positions
    ).astype(jnp.bfloat16)
    keys_and_values = jnp.concatenate([key_turned[:, 0, :], key_values[:, head_size:]], axis=1)
    start_state = (
        jnp.full((heads_here, query_rows), -1e30, jnp.float32),
        jnp.zeros((heads_here, query_rows), jnp.float32),
        jnp.zeros((heads_here, query_rows, head_size), jnp.float32),
    )
    top_all, total_all, acc_all = attend_keys(
        query_turned, head_size ** (-0.5), start_state, whole_of(keys_and_values, EP, (0, 1), 0)
    )
    head_out = (
        (acc_all / total_all[..., None])
        .transpose(1, 0, 2)
        .reshape(query_rows, heads_here * head_size)
        .astype(jnp.bfloat16)
    )
    tok_count = second_batch.shape[0]
    model_width = second_batch.shape[1]
    top_count = routes.shape[1]
    local_experts = expert_gate.shape[0]
    expert_count = local_experts * ep_count
    capacity = 3 * tok_count * top_count // (2 * expert_count)
    slot_count = expert_count * capacity
    token_float = second_batch.astype(jnp.float32)
    normed = (
        token_float
        * lax.rsqrt(jnp.mean(token_float * token_float, axis=-1, keepdims=True) + norm_eps)
        * norm_gain
    ).astype(jnp.bfloat16)
    own_slots = slot_ids(routes, expert_count, capacity)
    shared_hidden = (lambda pieces, begin_at: shared_hidden_of(pieces, shared_gate, shared_up))(
        gathered_copies(normed, "tp", 0), jnp.int32(0)
    )
    outgoing = jnp.take(
        normed, slot_table(own_slots, slot_count), axis=0, mode="fill", fill_value=0
    )[None]
    arrived = lax.all_to_all(outgoing, EP, split_axis=1, concat_axis=1, tiled=True)
    arrived = arrived.reshape(arrived.shape[0], ep_count, local_experts, capacity, model_width)
    hidden = expert_hidden(
        lax.all_gather(arrived, "tp", axis=0, tiled=True), expert_gate, expert_up
    )
    routed_part = jnp.einsum(
        "osjcf,jfd->osjcd", hidden, expert_down, preferred_element_type=jnp.float32
    ).reshape(-1, model_width)
    shared_part = jnp.dot(shared_hidden, shared_down, preferred_element_type=jnp.float32)
    head_partial = jnp.dot(head_out, out_weight, preferred_element_type=jnp.float32)
    attn_sum, routed_sum, shared_sum = (
        summed_on_arrival(head_partial.astype(jnp.bfloat16), "tp", 0),
        summed_on_arrival(routed_part.astype(jnp.bfloat16), "tp", 0),
        summed_on_arrival(shared_part.astype(jnp.bfloat16), "tp", 0),
    )
    returned = lax.all_to_all(
        routed_sum.astype(jnp.bfloat16), EP, split_axis=0, concat_axis=0, tiled=True
    )
    combined = shared_sum
    for slot_pick in range(top_count):
        combined = combined + route_weights[:, slot_pick : slot_pick + 1] * jnp.take(
            returned, own_slots[:, slot_pick], axis=0
        ).astype(jnp.float32)
    return (attn_sum.astype(jnp.bfloat16), combined.astype(jnp.bfloat16))


def solution(mesh):
    torus = Mesh(
        mesh.devices.reshape(mesh.shape["grp"], 16, 2, mesh.shape["tp"]),
        ("grp", "ep_0", "ep_1", "tp"),
    )
    return jax.shard_map(
        body,
        mesh=torus,
        in_specs=(
            P(GRP_EP, "tp"),
            P(GRP_EP, "tp"),
            P(),
            P(),
            P("tp", None),
            P(GRP_EP_TP, None),
            P(),
            P(GRP_EP_TP, None),
            P(GRP_EP_TP, None),
            P(EP, None, "tp"),
            P(EP, None, "tp"),
            P(EP, "tp", None),
            P(None, "tp"),
            P(None, "tp"),
            P("tp", None),
        ),
        out_specs=(P(GRP_EP_TP, None), P(GRP_EP_TP, None)),
        check_vma=False,
    )
```

profile of v0, /device:TPU:33, one launch (start us, length us, event | category | flops | bytes accessed | tf_op | source)
XLA Modules:
  0.0 621.9 jit_solution(13244901644372939689)
XLA Ops:
  12.2 3.3 gather_fusion
  15.5 1.6 bitcast_select_fusion
  17.1 4.1 copy.120
  21.7 12.4 %reduce.10 = bf16[384,2048]{1,0:T(8,128)(2,1)} reduce(bf16[384,1,2048]{2,1,0:T(2,128)(2,1)} %bitcast.152, bf16[]{:T(256)} %broadcast.416), dimensions={1}, to_apply=%bitcast.134.reduce_sub_computation | reduce | bytes 3145730
  34.1 5.2 reshape.492
  39.3 25.6 %all-to-all-start.3 = ((bf16[32,2,12288]{2,1,0:T(2,128)(2,1)}), bf16[32,2,12288]{2,1,0:T(2,128)(2,1)}, u32[]{:S(2)}, u32[]{:S(2)}) async-start(bf16[32,2,12288]{2,1,0:T(2,128)(2,1)} %reshape.492), calls=%async_computation.3 | async-start | bytes 3145728 | tf_op jit(solution)/shard_map/all_to_all | solution.py:220
  66.8 95.3 %all-gather.8.cloned.1.call-done = bf16[6144,128]{0,1:T(8,128)(2,1)} async-done(((bf16[384,128]{0,1:T(8,128)(2,1)}), bf16[6144,128]{0,1:T(8,128)(2,1)}) %all-gather.8.cloned.1.call-update) | async-done | bytes 1572880 | tf_op jit(solution)/shard_map/all_gather | solution.py:24
  162.1 2.6 copy.106
  164.9 9.5 %reshape.493 = bf16[384,1,2048]{2,1,0:T(2,128)(2,1)} reshape(bf16[32,2,12288]{2,1,0:T(2,128)(2,1)} %all-to-all-done.3) | data formatting | bytes 3145728
  174.3 12.2 %bitcast_reduce_fusion.2 = bf16[384,2048]{1,0:T(8,128)(2,1)} fusion(bf16[384,1,2048]{2,1,0:T(2,128)(2,1)} %reshape.493), kind=kLoop, calls=%fused_computation.129 | loop fusion | bytes 3145728 | tf_op jit(solution)/shard_map/all_to_all | solution.py:220
  186.6 3.7 reshape.450
  190.3 3.6 copy.99
  194.0 1.7 broadcast_in_dim.47
  195.7 4.8 all-to-all-start.1
  202.6 25.4 %all-to-all-done.1 = bf16[4,128,2048]{2,1,0:T(8,128)(2,1)} async-done(((bf16[4,128,2048]{2,1,0:T(8,128)(2,1)}), bf16[4,128,2048]{2,1,0:T(8,128)(2,1)}, u32[]{:S(2)}, u32[]{:S(2)}) %all-to-all-start.1) | async-done | bytes 2097184 | tf_op jit(solution)/shard_map/all_to_all | solution.py:37
  227.9 2.4 fusion.58
  230.3 5.5 convolution_convert_fusion
  235.8 4.5 all-to-all-start.2
  240.4 4.0 copy.91
  244.4 55.9 %all-gather.6.cloned.1.call-done = bf16[4,32,2,6,2048]{4,1,3,0,2:T(8,128)(2,1)} async-done(((bf16[1,32,2,6,2048]{4,1,3,0,2:T(8,128)(2,1)}), bf16[4,32,2,6,2048]{4,1,3,0,2:T(8,128)(2,1)}) %all-gather.6.cloned.1.call-update) | async-done | bytes 6291472 | tf_op jit(solution)/shard_map/all_gather | solution.py:223
  300.3 6.4 %fusion.14 = f32[2,4,32,6,256]{4,2,3,1,0:T(8,128)} fusion(bf16[4,32,2,6,2048]{4,1,3,0,2:T(8,128)(2,1)} %all-gather.6.cloned.1.call-done, bf16[2,2048,256]{2,1,0:T(8,128)(2,1)} %param.28), kind=kOutput, calls=%fused_computation.27 | convolution fusion | flops 1610612736 | bytes 9961472 | tf_op jit(solution)/shard_map/osjcd,jdf->osjcf/dot_general | solution.py:145
  306.7 10.1 %convert_bitcast_fusion = bf16[4,32,2,6,2048]{4,1,3,0,2:T(8,128)(2,1)} fusion(bf16[2,256,2048]{2,1,0:T(8,128)(2,1)S(1)} %copy-done, f32[2,4,32,6,256]{4,2,3,1,0:T(8,128)} %fusion.14, bf16[4,32,2,6,2048]{4,1,3,0,2:T(8,128)(2,1)} %all-gather.6.cloned.1.call-done, bf16[2,2048,256]{2,1,0:T(8,128)(2,1)} %param.29), kind=kOutput, calls=%fused_computation.20 | convolution fusion | flops 3226730496 | bytes 18350080 | tf_op jit(solution)/shard_map/osjcf,jfd->osjcd/dot_general | solution.py:225
  316.8 10.2 %copy.100 = bf16[4,32,2,6,2048]{4,0,3,2,1:T(4,128)(2,1)} copy(bf16[4,32,2,6,2048]{4,1,3,0,2:T(8,128)(2,1)} %convert_bitcast_fusion) | data formatting | bytes 12582912 | tf_op jit(solution)/shard_map/convert_element_type | solution.py:232
  327.0 9.1 %copy.101 = bf16[4,384,2048]{2,1,0:T(8,128)(2,1)} copy(bf16[4,384,2048]{2,0,1:T(4,128)(2,1)} %bitcast.151) | data formatting | bytes 12582912 | tf_op jit(solution)/shard_map/convert_element_type | solution.py:232
  336.1 5.3 all-to-all-start.4
  341.5 127.8 %while.15 = (s32[]{:T(128)}, f32[4,384]{1,0:T(4,128)S(1)}, f32[4,384]{1,0:T(4,128)S(1)}, f32[4,384,64]{1,2,0:T(8,128)S(1)}, bf16[12,1024,128]{2,1,0:T(8,128)(2,1...) while((s32[]{:T(128)}, f32[4,384]{1,0:T(4,128)S(1)}, f32[4,384]{1,0:T(4,128)S(1)}, ...), condition=%wide.region_5.6_spmd.clone, body=%wide.region_2.5_spmd.clone.sunk | while | flops 415538688 | bytes 46432384 | solution.py:134
  342.7 3.6 bitcast_reduce_fusion.4
  346.3 4.0 fusion.76
  353.3 3.6 bitcast_reduce_fusion.4
  357.0 4.0 fusion.76
  364.0 3.6 bitcast_reduce_fusion.4
  367.6 4.0 fusion.76
  372.2 1.3 fusion.78
  374.6 3.6 bitcast_reduce_fusion.4
  378.2 4.0 fusion.76
  382.8 1.3 fusion.78
  385.3 3.6 bitcast_reduce_fusion.4
  388.9 4.0 fusion.76
  395.9 3.6 bitcast_reduce_fusion.4
  399.5 4.0 fusion.76
  406.5 3.6 bitcast_reduce_fusion.4
  410.2 4.0 fusion.76
  417.2 3.6 bitcast_reduce_fusion.4
  420.8 4.0 fusion.76
  427.8 3.6 bitcast_reduce_fusion.4
  431.5 4.0 fusion.76
  438.5 3.6 bitcast_reduce_fusion.4
  442.1 4.0 fusion.76
  449.1 3.6 bitcast_reduce_fusion.4
  452.8 4.0 fusion.76
  459.8 3.6 bitcast_reduce_fusion.4
  463.4 4.0 fusion.76
  469.3 1.8 convolution_convert_fusion.1
  471.1 4.1 all-to-all-start
  475.3 5.7 reduce_sum.96
  480.9 3.6 all_to_all.28
  484.5 10.4 %all-to-all-done = bf16[4,96,2048]{2,1,0:T(8,128)(2,1)S(1)} async-done(((bf16[4,96,2048]{2,1,0:T(8,128)(2,1)}), bf16[4,96,2048]{2,1,0:T(8,128)(2,1)S(1)}, u32[]{:S(2)}, u32[]{:S(2)}) %all-to-all-start) | async-done | bytes 1572896 | tf_op jit(solution)/shard_map/all_to_all | solution.py:52
  495.0 11.2 %all-to-all-start.5 = ((bf16[32,12,2048]{2,1,0:T(8,128)(2,1)}), bf16[32,12,2048]{2,1,0:T(8,128)(2,1)}, u32[]{:S(2)}, u32[]{:S(2)}) async-start(bf16[32,12,2048]{2,1,0:T(8,128)(2,1)} %all_to_all.28), calls=%async_computation.5 | async-start | bytes 4194304 | tf_op jit(solution)/shard_map/all_to_all | solution.py:235
  506.4 2.1 convert_reduce_fusion
  509.6 94.8 %all-to-all-done.5 = bf16[32,12,2048]{2,1,0:T(8,128)(2,1)} async-done(((bf16[32,12,2048]{2,1,0:T(8,128)(2,1)}), bf16[32,12,2048]{2,1,0:T(8,128)(2,1)}, u32[]{:S(2)}, u32[]{:S(2)}) %all-to-all-start.5) | async-done | bytes 1572896 | tf_op jit(solution)/shard_map/all_to_all | solution.py:235
  604.4 2.5 all_to_all.30
  606.9 1.7 gather_fusion.1
  608.7 4.0 gather_fusion.2
  612.7 2.4 add_convert_fusion
  (180 shorter events, 44.5 us)
Async XLA Ops:
  7.2 299.5 %copy-start = (bf16[2,256,2048]{2,1,0:T(8,128)(2,1)S(1)}, bf16[2,256,2048]{2,1,0:T(8,128)(2,1)}, u32[]{:S(2)}) copy-start(bf16[2,256,2048]{2,1,0:T(8,128)(2,1)} %param.30) | copy-start | bytes 6291460
  39.3 25.7 %copy-start.5 = (bf16[384,128]{1,0:T(8,128)(2,1)S(1)}, bf16[384,128]{1,0:T(8,128)(2,1)}, u32[]{:S(2)}) copy-start(bf16[384,128]{1,0:T(8,128)(2,1)} %param.20) | copy-start | bytes 294916
  39.3 26.0 %copy-start.9 = (f32[64]{0:T(128)S(1)}, f32[64]{0:T(128)}, u32[]{:S(2)}) copy-start(f32[64]{0:T(128)} %param.22) | copy-start | bytes 772
  39.3 125.6 %all-to-all-start.3 = ((bf16[32,2,12288]{2,1,0:T(2,128)(2,1)}), bf16[32,2,12288]{2,1,0:T(2,128)(2,1)}, u32[]{:S(2)}, u32[]{:S(2)}) async-start(bf16[32,2,12288]{2,1,0:T(2,128)(2,1)} %reshape.492), calls=%async_computation.3 | async-start | bytes 3145728 | tf_op jit(solution)/shard_map/all_to_all | solution.py:220
  64.9 97.2 %all-gather.8.cloned.1.call-start = ((), (), s32[]{:S(2)}) async-start(), calls=%async_computation.7 | async-start | bytes 1671168 | tf_op jit(solution)/shard_map/all_gather | solution.py:24
  66.7 173.7 %all-gather.10.cloned.1.call-start = ((), (), s32[]{:S(2)}) async-start(), calls=%async_computation.8 | async-start | bytes 4718592 | tf_op jit(solution)/shard_map/all_gather | solution.py:24
  164.8 135.5 %all-gather.6.cloned.1.call-start = ((), (), s32[]{:S(2)}) async-start(), calls=%async_computation.6 | async-start | bytes 7864320 | tf_op jit(solution)/shard_map/all_gather | solution.py:223
  195.7 4.9 copy-start.6
  195.7 5.3 copy-start.10
  195.7 32.2 %all-to-all-start.1 = ((bf16[4,128,2048]{2,1,0:T(8,128)(2,1)}), bf16[4,128,2048]{2,1,0:T(8,128)(2,1)}, u32[]{:S(2)}, u32[]{:S(2)}) async-start(bf16[4,128,2048]{2,1,0:T(8,128)(2,1)} %broadcast_in_dim.47), calls=%async_computation.1 | async-start | bytes 4194304 | tf_op jit(solution)/shard_map/all_to_all | solution.py:37
  235.8 100.3 %all-to-all-start.2 = ((bf16[4,128,2048]{2,1,0:T(8,128)(2,1)}), bf16[4,128,2048]{2,1,0:T(8,128)(2,1)}, u32[]{:S(2)}, u32[]{:S(2)}) async-start(bf16[4,128,2048]{2,1,0:T(8,128)(2,1)} %bitcast.153), calls=%async_computation.2 | async-start | bytes 4194304 | tf_op jit(solution)/shard_map/all_to_all | solution.py:52
  336.1 135.0 %all-to-all-start.4 = ((bf16[4,384,2048]{2,1,0:T(8,128)(2,1)}), bf16[4,384,2048]{2,1,0:T(8,128)(2,1)}, u32[]{:S(2)}, u32[]{:S(2)}) async-start(bf16[4,384,2048]{2,1,0:T(8,128)(2,1)} %copy.101), calls=%async_computation.4 | async-start | bytes 12582912 | tf_op jit(solution)/shard_map/all_to_all | solution.py:52
  341.4 127.9 %copy-start.4 = (bf16[256,2048]{1,0:T(8,128)(2,1)S(1)}, bf16[256,2048]{1,0:T(8,128)(2,1)}, u32[]{:S(2)}) copy-start(bf16[256,2048]{1,0:T(8,128)(2,1)} %param.23) | copy-start | bytes 3145732
  346.3 4.6 copy-start.2
  357.0 4.6 copy-start.2
  367.6 4.6 copy-start.2
  378.2 4.6 copy-start.2
  388.9 4.6 copy-start.2
  399.5 4.6 copy-start.2
  410.2 4.6 copy-start.2
  420.8 4.6 copy-start.2
  431.5 4.6 copy-start.2
  442.1 4.6 copy-start.2
  452.7 4.6 copy-start.2
  463.4 4.6 copy-start.2
  471.1 23.9 %all-to-all-start = ((bf16[4,96,2048]{2,1,0:T(8,128)(2,1)}), bf16[4,96,2048]{2,1,0:T(8,128)(2,1)S(1)}, u32[]{:S(2)}, u32[]{:S(2)}) async-start(bf16[4,96,2048]{2,1,0:T(8,128)(2,1)} %bitcast.156), calls=%async_computation | async-start | bytes 3145728 | tf_op jit(solution)/shard_map/all_to_all | solution.py:52
  484.5 21.8 %copy-start.7 = (s32[128,2]{0,1:T(2,128)S(1)}, s32[128,2]{0,1:T(2,128)}, u32[]{:S(2)}) copy-start(s32[128,2]{0,1:T(2,128)} %param.26) | copy-start | bytes 3076
  484.5 21.9 %copy-start.8 = (f32[128,2]{0,1:T(2,128)S(1)}, f32[128,2]{0,1:T(2,128)}, u32[]{:S(2)}) copy-start(f32[128,2]{0,1:T(2,128)} %param.27) | copy-start | bytes 3076
  495.0 109.4 %all-to-all-start.5 = ((bf16[32,12,2048]{2,1,0:T(8,128)(2,1)}), bf16[32,12,2048]{2,1,0:T(8,128)(2,1)}, u32[]{:S(2)}, u32[]{:S(2)}) async-start(bf16[32,12,2048]{2,1,0:T(8,128)(2,1)} %all_to_all.28), calls=%async_computation.5 | async-start | bytes 4194304 | tf_op jit(solution)/shard_map/all_to_all | solution.py:235
  606.9 1.8 copy-start.3
  608.7 6.4 %copy-start.1 = (bf16[2,256,2048]{2,1,0:T(8,128)(2,1)S(1)}, bf16[2,256,2048]{2,1,0:T(8,128)(2,1)}, u32[]{:S(2)}) copy-start(bf16[2,256,2048]{2,1,0:T(8,128)(2,1)} %param.30) | copy-start | bytes 6291460
Sparse Core Ops, SparseCore 0:
  68.1 93.9 all-gather.7
  164.9 24.2 all-gather.9
  194.1 106.1 all-gather.5
where the time goes:
time: 626 us; the launch traced here: 622 us
  waiting for transfers between devices  282 us (45%)
  local copies, waits for them, and re-layouts  105 us (17%)
  matrix products  84.7 us (14%)
  other arithmetic  79.3 us (13%)
  starting transfers between devices  55.8 us (9%)
  between operations  14.5 us (2%)
    all_gather x2, waiting for transfers between devices, stacked_from(): tiles = lax.all_gather(tiles, axes[k])  95.4 us
    all_to_all x1, waiting for transfers between devices, body(): lax.all_to_all(routed_sum.astype(jnp.bfloat16), EP, split_axis=0, concat_...  94.8 us
    all_gather x1, waiting for transfers between devices, body(): lax.all_gather(arrived, 'tp', axis=0, tiled=True)  55.9 us
    reduce_sum x12, other arithmetic, one_block(): total_new = total_now * shrink + jnp.sum(exps, axis=-1)  47.6 us
    dot_general x12, matrix products, one_block(): jnp.einsum('qhd,kd->hqk', query_turned, block_rows[:, :head_size], prefer...  43.5 us
    all_to_all x1, starting transfers between devices, body(): lax.all_to_all(outgoing, EP, split_axis=1, concat_axis=1, tiled=True)  25.6 us
    all_to_all x1, waiting for transfers between devices, from_everyone(): return lax.all_to_all(copies, axis, split_axis=0, concat_axis=0, tiled=True)  25.4 us
    convert_element_type x2, local copies, waits for them, and re-layouts, body(): routed_part.astype(jnp.bfloat16)  19.3 us
  transfers between devices with their start and end apart: 9, of which 5 were waited for; matrix products, arithmetic and copies ran while one was open for 35% of the time, Pallas kernels for 0%

commit v1 on v0

--- a/solution.py
+++ b/solution.py
@@ -220,7 +220,11 @@
     arrived = lax.all_to_all(outgoing, EP, split_axis=1, concat_axis=1, tiled=True)
     arrived = arrived.reshape(arrived.shape[0], ep_count, local_experts, capacity, model_width)
     hidden = expert_hidden(
-        lax.all_gather(arrived, "tp", axis=0, tiled=True), expert_gate, expert_up
+        jnp.concatenate(
+            lax.all_to_all(jnp.stack([arrived] * lax.axis_size("tp")), "tp", 0, 0), axis=0
+        ),
+        expert_gate,
+        expert_up,
     )
     routed_part = jnp.einsum(
         "osjcf,jfd->osjcd", hidden, expert_down, preferred_element_type=jnp.float32

time: 626 us -> 589 us (0.941)
  waiting for transfers between devices: 282 us -> 238 us
    all_to_all x1, waiting for transfers between devices: 0.01 us -> 77 us  [body(): lax.all_to_all(outgoing, EP, split_axis=1, concat_axis=1, tiled=True)]
    all_gather x2, waiting for transfers between devices: 95.4 us -> 35 us  [stacked_from(): tiles = lax.all_gather(tiles, axes[k])]
    all_gather x1 -> x0, waiting for transfers between devices: 55.9 us -> none  [body(): lax.all_gather(arrived, 'tp', axis=0, tiled=True)]
    all_to_all x1, waiting for transfers between devices: 25.4 us -> 0.01 us  [from_everyone(): return lax.all_to_all(copies, axis, split_axis=0, concat_axis=0, tiled=True)]
    all_to_all x0 -> x1, waiting for transfers between devices: none -> 19.2 us  [body(): lax.all_to_all(jnp.stack([arrived] * lax.axis_size('tp')), 'tp', 0, 0)]
    another operation x1 -> x4, local copies, waits for them, and re-layouts: 0.01 us -> 12.6 us  [the longest x3 12.6 us: body(): jnp.stack([arrived] * lax.axis_size('tp'))]
    reshape x2 -> x0, local copies, waits for them, and re-layouts: 7.34 us -> none  [body(): arrived.reshape(arrived.shape[0], ep_count, local_experts, capacity, mode...]
  transfers between devices with their start and end apart: 9 -> 9, of which waited for: 5 -> 6; matrix products, arithmetic and copies ran while one was open for 35% -> 37% of each run, Pallas kernels for 0% -> 0%
where the time goes in v1:
time: 589 us; the launch traced here: 584 us
  waiting for transfers between devices  238 us (40%)
  local copies, waits for them, and re-layouts  110 us (19%)
  matrix products  84.7 us (14%)
  other arithmetic  79.3 us (13%)
  starting transfers between devices  57.1 us (10%)
  between operations  14.7 us (2%)
    all_to_all x1, waiting for transfers between devices, body(): lax.all_to_all(routed_sum.astype(jnp.bfloat16), EP, split_axis=0, concat_...  96.8 us
    all_to_all x1, waiting for transfers between devices, body(): lax.all_to_all(outgoing, EP, split_axis=1, concat_axis=1, tiled=True)  77 us
    reduce_sum x12, other arithmetic, one_block(): total_new = total_now * shrink + jnp.sum(exps, axis=-1)  47.6 us
    dot_general x12, matrix products, one_block(): jnp.einsum('qhd,kd->hqk', query_turned, block_rows[:, :head_size], prefer...  43.5 us
    all_gather x2, waiting for transfers between devices, stacked_from(): tiles = lax.all_gather(tiles, axes[k])  35 us
    all_to_all x1, starting transfers between devices, body(): lax.all_to_all(outgoing, EP, split_axis=1, concat_axis=1, tiled=True)  25.6 us
    convert_element_type x2, local copies, waits for them, and re-layouts, body(): routed_part.astype(jnp.bfloat16)  19.3 us
    all_to_all x1, waiting for transfers between devices, body(): lax.all_to_all(jnp.stack([arrived] * lax.axis_size('tp')), 'tp', 0, 0)  19.2 us
  transfers between devices with their start and end apart: 9, of which 6 were waited for; matrix products, arithmetic and copies ran while one was open for 37% of the time, Pallas kernels for 0%

profile of v1, /device:TPU:33, one launch (start us, length us, event | category | flops | bytes accessed | tf_op | source)
XLA Modules:
  0.0 584.1 jit_solution(6906188248415132187)
XLA Ops:
  12.2 3.3 gather_fusion
  17.1 4.1 copy.136
  21.7 12.4 %reduce.10 = bf16[384,2048]{1,0:T(8,128)(2,1)} reduce(bf16[384,1,2048]{2,1,0:T(2,128)(2,1)} %bitcast.159, bf16[]{:T(256)} %broadcast.418), dimensions={1}, to_apply=%bitcast.141.reduce_sub_computation | reduce | bytes 3145730
  34.1 5.0 reshape.496
  39.1 25.6 %all-to-all-start.3 = ((bf16[32,2,12288]{2,1,0:T(2,128)(2,1)}), bf16[32,2,12288]{2,1,0:T(2,128)(2,1)}, u32[]{:S(2)}, u32[]{:S(2)}) async-start(bf16[32,2,12288]{2,1,0:T(2,128)(2,1)} %reshape.496), calls=%async_computation.3 | async-start | bytes 3145728 | tf_op jit(solution)/shard_map/all_to_all | solution.py:220
  65.5 77.0 %all-to-all-done.3 = bf16[32,2,12288]{2,1,0:T(2,128)(2,1)} async-done(((bf16[32,2,12288]{2,1,0:T(2,128)(2,1)}), bf16[32,2,12288]{2,1,0:T(2,128)(2,1)}, u32[]{:S(2)}, u32[]{:S(2)}) %all-to-all-start.3) | async-done | bytes 1572896 | tf_op jit(solution)/shard_map/all_to_all | solution.py:220
  142.6 1.6 broadcast_in_dim.47
  144.2 4.5 all-to-all-start.1
  149.7 9.5 %reshape.497 = bf16[384,1,2048]{2,1,0:T(2,128)(2,1)} reshape(bf16[32,2,12288]{2,1,0:T(2,128)(2,1)} %all-to-all-done.3) | data formatting | bytes 3145728
  159.2 12.2 %bitcast_reduce_fusion.2 = bf16[384,2048]{1,0:T(8,128)(2,1)} fusion(bf16[384,1,2048]{2,1,0:T(2,128)(2,1)} %reshape.497), kind=kLoop, calls=%fused_computation.133 | loop fusion | bytes 3145728 | tf_op jit(solution)/shard_map/all_to_all | solution.py:220
  171.5 4.1 stack_reshape.2
  175.6 3.6 copy.102
  179.2 4.9 stack.17
  184.1 5.3 all-to-all-start.4
  189.5 16.3 %all-gather.5.cloned.1.call-done = bf16[6144,128]{0,1:T(8,128)(2,1)} async-done(((bf16[384,128]{0,1:T(8,128)(2,1)}), bf16[6144,128]{0,1:T(8,128)(2,1)}) %all-gather.5.cloned.1.call-update) | async-done | bytes 1572880 | tf_op jit(solution)/shard_map/all_gather | solution.py:24
  205.8 2.6 copy.110
  210.5 2.4 fusion.66
  212.9 5.5 convolution_convert_fusion
  218.4 18.7 %all-gather.7.cloned.1.call-done = bf16[32,384,128]{2,1,0:T(8,128)(2,1)} async-done(((bf16[16,384,128]{2,1,0:T(8,128)(2,1)}), bf16[32,384,128]{2,1,0:T(8,128)(2,1)}) %all-gather.7.cloned.1.call-update) | async-done | bytes 3145744 | tf_op jit(solution)/shard_map/all_gather | solution.py:24
  237.1 3.9 copy.94
  241.0 19.2 %all-to-all-done.4 = bf16[4,1,32,2,6,2048]{5,2,4,3,1,0:T(8,128)(2,1)} async-done(((bf16[4,1,32,2,6,2048]{5,2,4,3,1,0:T(8,128)(2,1)}), bf16[4,1,32,2,6,2048]{5,2,4,3,1,0:T(8,128)(2,1)}, u32[]{:S(2)}, u32[]{:S(2)}) %all-to-all-start.4) | async-done | bytes 6291488 | tf_op jit(solution)/shard_map/all_to_all | solution.py:224
  260.2 4.7 all-to-all-start.2
  265.0 6.4 %fusion.13 = f32[2,4,32,6,256]{4,2,3,1,0:T(8,128)} fusion(bf16[4,1,32,2,6,2048]{5,2,4,3,1,0:T(8,128)(2,1)} %all-to-all-done.4, bf16[2,2048,256]{2,1,0:T(8,128)(2,1)} %param.28), kind=kOutput, calls=%fused_computation.22 | convolution fusion | flops 1610612736 | bytes 9961472 | tf_op jit(solution)/shard_map/osjcd,jdf->osjcf/dot_general | solution.py:145
  271.4 10.1 %convert_bitcast_fusion = bf16[4,32,2,6,2048]{4,1,3,0,2:T(8,128)(2,1)} fusion(bf16[2,256,2048]{2,1,0:T(8,128)(2,1)S(1)} %copy-done, f32[2,4,32,6,256]{4,2,3,1,0:T(8,128)} %fusion.13, bf16[2,2048,256]{2,1,0:T(8,128)(2,1)} %param.29, bf16[4,1,32,2,6,2048]{5,2,4,3,1,0:T(8,128)(2,1)} %all-to-all-done.4), kind=kOutput, calls=%fused_computation.24 | convolution fusion | flops 3226730496 | bytes 18350080 | tf_op jit(solution)/shard_map/osjcf,jfd->osjcd/dot_general | solution.py:229
  281.4 10.2 %copy.104 = bf16[4,32,2,6,2048]{4,0,3,2,1:T(4,128)(2,1)} copy(bf16[4,32,2,6,2048]{4,1,3,0,2:T(8,128)(2,1)} %convert_bitcast_fusion) | data formatting | bytes 12582912 | tf_op jit(solution)/shard_map/convert_element_type | solution.py:236
  291.7 9.1 %copy.105 = bf16[4,384,2048]{2,1,0:T(8,128)(2,1)} copy(bf16[4,384,2048]{2,0,1:T(4,128)(2,1)} %bitcast.158) | data formatting | bytes 12582912 | tf_op jit(solution)/shard_map/convert_element_type | solution.py:236
  300.8 5.3 all-to-all-start.5
  306.1 127.8 %while.15 = (s32[]{:T(128)}, f32[4,384]{1,0:T(4,128)S(1)}, f32[4,384]{1,0:T(4,128)S(1)}, f32[4,384,64]{1,2,0:T(8,128)S(1)}, bf16[12,1024,128]{2,1,0:T(8,128)(2,1...) while((s32[]{:T(128)}, f32[4,384]{1,0:T(4,128)S(1)}, f32[4,384]{1,0:T(4,128)S(1)}, ...), condition=%wide.region_5.6_spmd.clone, body=%wide.region_2.5_spmd.clone.sunk | while | flops 415538688 | bytes 46432384 | solution.py:134
  307.4 3.6 bitcast_reduce_fusion.4
  311.0 4.0 fusion.82
  318.0 3.6 bitcast_reduce_fusion.4
  321.6 4.0 fusion.82
  328.6 3.6 bitcast_reduce_fusion.4
  332.3 4.0 fusion.82
  339.3 3.6 bitcast_reduce_fusion.4
  342.9 4.0 fusion.82
  349.9 3.6 bitcast_reduce_fusion.4
  353.6 4.0 fusion.82
  360.6 3.6 bitcast_reduce_fusion.4
  364.2 4.0 fusion.82
  371.2 3.6 bitcast_reduce_fusion.4
  374.9 4.0 fusion.82
  381.9 3.6 bitcast_reduce_fusion.4
  385.5 4.0 fusion.82
  392.5 3.6 bitcast_reduce_fusion.4
  396.1 4.0 fusion.82
  403.2 3.6 bitcast_reduce_fusion.4
  406.8 4.0 fusion.82
  413.8 3.6 bitcast_reduce_fusion.4
  417.4 4.0 fusion.82
  424.4 3.6 bitcast_reduce_fusion.4
  428.1 4.0 fusion.82
  434.0 1.8 convolution_convert_fusion.1
  435.8 4.1 all-to-all-start
  439.9 5.7 reduce_sum.96
  445.6 3.6 all_to_all.32
  449.2 9.6 %all-to-all-done = bf16[4,96,2048]{2,1,0:T(8,128)(2,1)S(1)} async-done(((bf16[4,96,2048]{2,1,0:T(8,128)(2,1)}), bf16[4,96,2048]{2,1,0:T(8,128)(2,1)S(1)}, u32[]{:S(2)}, u32[]{:S(2)}) %all-to-all-start) | async-done | bytes 1572896 | tf_op jit(solution)/shard_map/all_to_all | solution.py:52
  458.8 7.3 %all-to-all-start.6 = ((bf16[32,12,2048]{2,1,0:T(8,128)(2,1)}), bf16[32,12,2048]{2,1,0:T(8,128)(2,1)}, u32[]{:S(2)}, u32[]{:S(2)}) async-start(bf16[32,12,2048]{2,1,0:T(8,128)(2,1)} %all_to_all.32), calls=%async_computation.6 | async-start | bytes 4194304 | tf_op jit(solution)/shard_map/all_to_all | solution.py:239
  466.4 2.1 convert_reduce_fusion
  469.6 96.8 %all-to-all-done.6 = bf16[32,12,2048]{2,1,0:T(8,128)(2,1)} async-done(((bf16[32,12,2048]{2,1,0:T(8,128)(2,1)}), bf16[32,12,2048]{2,1,0:T(8,128)(2,1)}, u32[]{:S(2)}, u32[]{:S(2)}) %all-to-all-start.6) | async-done | bytes 1572896 | tf_op jit(solution)/shard_map/all_to_all | solution.py:239
  566.4 2.5 all_to_all.34
  568.9 1.7 gather_fusion.1
  570.6 4.0 gather_fusion.2
  574.6 2.4 add_convert_fusion
  (180 shorter events, 48.5 us)
Async XLA Ops:
  7.2 264.2 %copy-start = (bf16[2,256,2048]{2,1,0:T(8,128)(2,1)S(1)}, bf16[2,256,2048]{2,1,0:T(8,128)(2,1)}, u32[]{:S(2)}) copy-start(bf16[2,256,2048]{2,1,0:T(8,128)(2,1)} %param.30) | copy-start | bytes 6291460
  39.1 25.6 %copy-start.5 = (bf16[384,128]{1,0:T(8,128)(2,1)S(1)}, bf16[384,128]{1,0:T(8,128)(2,1)}, u32[]{:S(2)}) copy-start(bf16[384,128]{1,0:T(8,128)(2,1)} %param.20) | copy-start | bytes 294916
  39.1 25.9 %copy-start.9 = (f32[64]{0:T(128)S(1)}, f32[64]{0:T(128)}, u32[]{:S(2)}) copy-start(f32[64]{0:T(128)} %param.22) | copy-start | bytes 772
  39.1 103.5 %all-to-all-start.3 = ((bf16[32,2,12288]{2,1,0:T(2,128)(2,1)}), bf16[32,2,12288]{2,1,0:T(2,128)(2,1)}, u32[]{:S(2)}, u32[]{:S(2)}) async-start(bf16[32,2,12288]{2,1,0:T(2,128)(2,1)} %reshape.496), calls=%async_computation.3 | async-start | bytes 3145728 | tf_op jit(solution)/shard_map/all_to_all | solution.py:220
  144.2 34.9 %all-to-all-start.1 = ((bf16[4,128,2048]{2,1,0:T(8,128)(2,1)}), bf16[4,128,2048]{2,1,0:T(8,128)(2,1)}, u32[]{:S(2)}, u32[]{:S(2)}) async-start(bf16[4,128,2048]{2,1,0:T(8,128)(2,1)} %broadcast_in_dim.47), calls=%async_computation.1 | async-start | bytes 4194304 | tf_op jit(solution)/shard_map/all_to_all | solution.py:37
  148.8 57.0 %all-gather.5.cloned.1.call-start = ((), (), s32[]{:S(2)}) async-start(), calls=%async_computation.7 | async-start | bytes 1671168 | tf_op jit(solution)/shard_map/all_gather | solution.py:24
  184.1 76.2 %all-to-all-start.4 = ((bf16[4,1,32,2,6,2048]{5,2,4,3,1,0:T(8,128)(2,1)}), bf16[4,1,32,2,6,2048]{5,2,4,3,1,0:T(8,128)(2,1)}, u32[]{:S(2)}, u32[]{:S(2)}) async-start(bf16[4,1,32,2,6,2048]{5,2,4,3,1,0:T(8,128)(2,1)} %stack.17), calls=%async_computation.4 | async-start | bytes 12582912 | tf_op jit(solution)/shard_map/all_to_all | solution.py:224
  189.4 19.1 %copy-start.6 = (bf16[384,256]{1,0:T(8,128)(2,1)S(1)}, bf16[384,256]{1,0:T(8,128)(2,1)}, u32[]{:S(2)}) copy-start(bf16[384,256]{1,0:T(8,128)(2,1)} %param.19) | copy-start | bytes 589828
  189.4 19.5 %copy-start.10 = (f32[64]{0:T(128)S(1)}, f32[64]{0:T(128)}, u32[]{:S(2)}) copy-start(f32[64]{0:T(128)} %param.21) | copy-start | bytes 772
  189.4 47.7 %all-gather.7.cloned.1.call-start = ((), (), s32[]{:S(2)}) async-start(), calls=%async_computation.8 | async-start | bytes 4718592 | tf_op jit(solution)/shard_map/all_gather | solution.py:24
  260.2 40.6 %all-to-all-start.2 = ((bf16[4,128,2048]{2,1,0:T(8,128)(2,1)}), bf16[4,128,2048]{2,1,0:T(8,128)(2,1)}, u32[]{:S(2)}, u32[]{:S(2)}) async-start(bf16[4,128,2048]{2,1,0:T(8,128)(2,1)} %bitcast.160), calls=%async_computation.2 | async-start | bytes 4194304 | tf_op jit(solution)/shard_map/all_to_all | solution.py:52
  300.8 135.0 %all-to-all-start.5 = ((bf16[4,384,2048]{2,1,0:T(8,128)(2,1)}), bf16[4,384,2048]{2,1,0:T(8,128)(2,1)}, u32[]{:S(2)}, u32[]{:S(2)}) async-start(bf16[4,384,2048]{2,1,0:T(8,128)(2,1)} %copy.105), calls=%async_computation.5 | async-start | bytes 12582912 | tf_op jit(solution)/shard_map/all_to_all | solution.py:52
  306.1 127.9 %copy-start.4 = (bf16[256,2048]{1,0:T(8,128)(2,1)S(1)}, bf16[256,2048]{1,0:T(8,128)(2,1)}, u32[]{:S(2)}) copy-start(bf16[256,2048]{1,0:T(8,128)(2,1)} %param.23) | copy-start | bytes 3145732
  311.0 4.6 copy-start.2
  321.6 4.6 copy-start.2
  332.3 4.6 copy-start.2
  342.9 4.6 copy-start.2
  353.6 4.6 copy-start.2
  364.2 4.6 copy-start.2
  374.9 4.6 copy-start.2
  385.5 4.6 copy-start.2
  396.1 4.6 copy-start.2
  406.8 4.6 copy-start.2
  417.4 4.6 copy-start.2
  428.1 4.6 copy-start.2
  435.8 23.0 %all-to-all-start = ((bf16[4,96,2048]{2,1,0:T(8,128)(2,1)}), bf16[4,96,2048]{2,1,0:T(8,128)(2,1)S(1)}, u32[]{:S(2)}, u32[]{:S(2)}) async-start(bf16[4,96,2048]{2,1,0:T(8,128)(2,1)} %bitcast.163), calls=%async_computation | async-start | bytes 3145728 | tf_op jit(solution)/shard_map/all_to_all | solution.py:52
  449.2 17.1 %copy-start.7 = (s32[128,2]{0,1:T(2,128)S(1)}, s32[128,2]{0,1:T(2,128)}, u32[]{:S(2)}) copy-start(s32[128,2]{0,1:T(2,128)} %param.26) | copy-start | bytes 3076
  449.2 17.2 %copy-start.8 = (f32[128,2]{0,1:T(2,128)S(1)}, f32[128,2]{0,1:T(2,128)}, u32[]{:S(2)}) copy-start(f32[128,2]{0,1:T(2,128)} %param.27) | copy-start | bytes 3076
  458.8 107.6 %all-to-all-start.6 = ((bf16[32,12,2048]{2,1,0:T(8,128)(2,1)}), bf16[32,12,2048]{2,1,0:T(8,128)(2,1)}, u32[]{:S(2)}, u32[]{:S(2)}) async-start(bf16[32,12,2048]{2,1,0:T(8,128)(2,1)} %all_to_all.32), calls=%async_computation.6 | async-start | bytes 4194304 | tf_op jit(solution)/shard_map/all_to_all | solution.py:239
  568.9 1.8 copy-start.3
  570.6 6.4 %copy-start.1 = (bf16[2,256,2048]{2,1,0:T(8,128)(2,1)S(1)}, bf16[2,256,2048]{2,1,0:T(8,128)(2,1)}, u32[]{:S(2)}) copy-start(bf16[2,256,2048]{2,1,0:T(8,128)(2,1)} %param.30) | copy-start | bytes 6291460
Sparse Core Ops, SparseCore 0:
  152.0 53.7 all-gather.4
  208.6 28.4 all-gather.6
